TPU v7x, 32 devices: a whole 2x2x4 slice. The times are simulated.
32 devices in a mesh: grp: 2 (over y), sp: 4 (over z), tp: 4 (over x, core).
Axes of the slice: x: 2, y: 2, z: 4, core: 2. Of those that a mesh axis runs over, the one named last changes fastest.
Arguments:
- query_latent: bfloat16 [1024, 768], P(('grp', 'sp')), parts along dimension 0, may hold values from -6 to 6
- key_latent: bfloat16 [1024, 256], P(('grp', 'sp', 'tp')), parts along dimension 0, may hold values from -20 to 20
- rotary_key: bfloat16 [1024, 64], P(('grp', 'sp', 'tp')), parts along dimension 0, may hold values from -1000 to 1000
- query_gain: float32 [768], replicated, may hold values from 0.1 to 1.9
- latent_gain: float32 [256], replicated, may hold values from 0.1 to 1.9
- query_up: bfloat16 [768, 3072], P(None, 'tp'), may hold values from -0.21875 to 0.21875
- key_up: bfloat16 [256, 2048], P(None, 'tp'), may hold values from -0.375 to 0.375
- value_up: bfloat16 [256, 2048], P(None, 'tp'), may hold values from -0.375 to 0.375
- out_gain: float32 [2048], P('tp'), may hold values from 0.1 to 1.9
- out_weight: bfloat16 [2048, 4096], P('sp', 'tp'), may hold values from -0.125 to 0.125
Outputs:
- mixed: bfloat16 [1024, 4096], P(('grp', 'sp'), 'tp'), parts along dimension 0
There are 2 independent parts, one for each index of `grp`. A program takes and returns all parts, laid end to end along the dimension named above; an argument that names none is the same for every part. Nothing has to cross between parts.
All inputs are finite; a program needn't handle non-finite values.
Results may differ from a plain program's by a relative error of at most 0.02.
The roundings to bfloat16 on the way count: a program that leaves them out, or rounds other values in their place, can miss the bound.
Values may be sent and summed in bfloat16 or wider, within the bound.
A program may use at most 128 MiB of HBM per device.

v0:
```python
import jax
import jax.numpy as jnp
from jax import lax
from jax.sharding import PartitionSpec as P

HEADS = 16
NOPE_DIM = 128
ROPE_DIM = 64
VALUE_DIM = 128
KVRANK = 256


norm_eps = 1e-06
rope_theta = 10000.0


def rms_scaled(inputs, gain_vec):
    widened = inputs.astype(jnp.float32)
    return (
        widened
        * lax.rsqrt(jnp.mean(widened * widened, axis=-1, keepdims=True) + norm_eps)
        * gain_vec
    )


def rotate_half(inputs, positions):
    half_width = inputs.shape[-1] // 2
    inverse = rope_theta ** (-jnp.arange(half_width, dtype=jnp.float32) / half_width)
    angles = positions[:, None] * inverse[None, :]
    if inputs.ndim == 3:
        angles = angles[:, None, :]
    cosine = jnp.cos(angles)
    sine = jnp.sin(angles)
    widened = inputs.astype(jnp.float32)
    first = widened[..., :half_width]
    second = widened[..., half_width:]
    return jnp.concatenate(
        [first * cosine - second * sine, second * cosine + first * sine], axis=-1
    )


def on_device(
    query_latent,
    key_latent,
    rotary_key,
    query_gain,
    latent_gain,
    query_up,
    key_up,
    value_up,
    out_gain,
    out_weight,
):
    block_rows = query_latent.shape[0]
    row_count = key_latent.shape[0]
    head_local = key_up.shape[1] // NOPE_DIM
    block_start = lax.axis_index("sp") * block_rows
    own_start = block_start + lax.axis_index("tp") * row_count
    score_scale = (NOPE_DIM + ROPE_DIM) ** (-0.5)
    normed = rms_scaled(query_latent, query_gain).astype(jnp.bfloat16)
    query_full = jnp.dot(normed, query_up, preferred_element_type=jnp.float32).astype(jnp.bfloat16)
    query_full = query_full.reshape(block_rows, head_local, NOPE_DIM + ROPE_DIM)
    query_positions = (block_start + jnp.arange(block_rows, dtype=jnp.int32)).astype(jnp.float32)
    query_plain = query_full[..., :NOPE_DIM]
    query_turned = rotate_half(query_full[..., NOPE_DIM:], query_positions).astype(jnp.bfloat16)
    latent_normed = rms_scaled(key_latent, latent_gain).astype(jnp.bfloat16)
    own_positions = (own_start + jnp.arange(row_count, dtype=jnp.int32)).astype(jnp.float32)
    key_turned = rotate_half(rotary_key, own_positions).astype(jnp.bfloat16)
    running_max = jnp.full((block_rows, head_local), -1e30, jnp.float32)
    running_sum = jnp.zeros((block_rows, head_local), jnp.float32)
    weighted = jnp.zeros((block_rows, head_local, KVRANK), jnp.float32)
    latents = lax.all_gather(latent_normed, ("sp", "tp"), axis=0, tiled=True)
    turned_keys = lax.all_gather(key_turned, ("sp", "tp"), axis=0, tiled=True)
    portion_rows = latents.shape[0]
    step_rows = min(portion_rows, 2048)
    for begin in range(0, portion_rows, step_rows):
        latent_part = latents[begin : begin + step_rows]
        turned_part = turned_keys[begin : begin + step_rows]
        key_plain = jnp.dot(latent_part, key_up, preferred_element_type=jnp.float32).astype(
            jnp.bfloat16
        )
        key_plain = key_plain.reshape(latent_part.shape[0], head_local, NOPE_DIM)
        scores = jnp.einsum(
            "qhd,khd->qhk", query_plain, key_plain, preferred_element_type=jnp.float32
        )
        scores = scores + jnp.einsum(
            "qhd,kd->qhk", query_turned, turned_part, preferred_element_type=jnp.float32
        )
        scores = scores * score_scale
        new_max = jnp.maximum(running_max, jnp.max(scores, axis=-1))
        rescale = jnp.exp(running_max - new_max)
        expo = jnp.exp(scores - new_max[..., None])
        running_sum = running_sum * rescale + jnp.sum(expo, axis=-1)
        weighted = weighted * rescale[..., None] + jnp.einsum(
            "qhk,kc->qhc",
            expo.astype(jnp.bfloat16),
            latent_part,
            preferred_element_type=jnp.float32,
        )
        running_max = new_max
    final_state = (running_max, running_sum, weighted)
    running_max, running_sum, weighted = final_state
    latent_mix = (weighted / running_sum[..., None]).astype(jnp.bfloat16)
    value_heads = value_up.reshape(KVRANK, head_local, VALUE_DIM)
    head_out = jnp.einsum(
        "qhc,chd->qhd", latent_mix, value_heads, preferred_element_type=jnp.float32
    ).astype(jnp.bfloat16)
    head_out = head_out.reshape(block_rows, head_local * VALUE_DIM)
    widened = head_out.astype(jnp.float32)
    square_part = jnp.sum(widened * widened, axis=1)
    gained = (widened * out_gain).astype(jnp.bfloat16)
    all_gained, square_parts = (
        lax.all_gather(gained, "tp", axis=1, tiled=True),
        lax.all_gather(square_part[:, None].astype(jnp.bfloat16), "tp", axis=1, tiled=True).astype(
            jnp.float32
        ),
    )
    all_squares = jnp.sum(square_parts, axis=1)
    own_sums = jnp.dot(
        all_gained,
        lax.all_gather(out_weight, "sp", axis=0, tiled=True),
        preferred_element_type=jnp.float32,
    )
    mean_square = all_squares / (HEADS * VALUE_DIM)
    return (own_sums * lax.rsqrt(mean_square + norm_eps)[:, None]).astype(jnp.bfloat16)


def solution(mesh):
    in_specs = (
        P(("grp", "sp"), None),
        P(("grp", "sp", "tp"), None),
        P(("grp", "sp", "tp"), None),
        P(),
        P(),
        P(None, "tp"),
        P(None, "tp"),
        P(None, "tp"),
        P("tp"),
        P("sp", "tp"),
    )
    out_specs = P(("grp", "sp"), "tp")
    return jax.shard_map(
        on_device, mesh=mesh, in_specs=in_specs, out_specs=out_specs, check_vma=False
    )
```

profile of v0, /device:TPU:0, one launch (start us, length us, event | category | flops | bytes accessed | tf_op | source)
XLA Modules:
  0.0 103.9 jit_solution(13197024730950181628)
XLA Ops:
  6.5 0.7 all-gather.3.cloned.1.call-update
  7.3 1.0 %fusion.13 = f32[128]{0:T(128)S(1)} fusion(bf16[128,768]{1,0:T(8,128)(2,1)} %param.10), kind=kLoop, calls=%fused_computation.19 | loop fusion | flops 294784 | bytes 197120 | tf_op jit(solution)/shard_map/reduce_sum | solution.py:21
  8.3 1.3 %convolution_convert_fusion.1 = bf16[128,768]{1,0:T(8,128)(2,1)S(1)} fusion(bf16[768,768]{1,0:T(8,128)(2,1)S(1)} %copy-done, bf16[128,768]{1,0:T(8,128)(2,1)} %param.10, f32[768]{0:T(1024)} %param.13, f32[128]{0:T(128)S(1)} %add_rsqrt_fusion.1), kind=kOutput, calls=%fused_computation.9 | convolution fusion | flops 151486464 | bytes 1576448 | tf_op jit(solution)/shard_map/dot_general | solution.py:61
  9.6 0.2 copy.21
  9.8 0.7 convert_element_type.94
  10.5 1.1 %copy.30 = bf16[256,512]{0,1:T(8,128)(2,1)S(1)} copy(bf16[256,512]{1,0:T(8,128)(2,1)} %param.17) | data formatting | bytes 524288 | tf_op jit(solution)/shard_map/reshape | solution.py:104
  11.6 0.1 fusion.37
  11.8 0.1 pad_maximum_fusion
  11.8 24.3 %all_gather.16 = bf16[512,64]{1,0:T(8,128)(2,1)S(1)} all-gather(bf16[32,64]{1,0:T(8,128)(2,1)S(1)} %pad_maximum_fusion), channel_id=1, replica_groups=mesh['grp'=2,'sp'=4,'tp'=4] {'sp','tp'}, dimensions={0}, use_global_device_ids=true | all-gather | bytes 69632 | tf_op jit(solution)/shard_map/all_gather | solution.py:73
  36.2 0.8 fusion.29
  37.0 0.8 fusion.31
  37.8 20.0 %all_gather.15 = bf16[512,256]{1,0:T(8,128)(2,1)S(1)} all-gather(bf16[32,256]{1,0:T(8,128)(2,1)S(1)} %fusion.31), channel_id=1, replica_groups=mesh['grp'=2,'sp'=4,'tp'=4] {'sp','tp'}, dimensions={0}, use_global_device_ids=true | all-gather | bytes 278528 | tf_op jit(solution)/shard_map/all_gather | solution.py:72
  57.9 0.1 multiply_cosine_fusion.1
  58.1 0.3 convolution_convert_fusion
  58.4 0.0 copy-start.2
  58.4 0.3 convolution_bitcast_fusion
  58.8 0.3 fusion.42
  59.1 0.2 fusion.7
  59.2 0.6 multiply_reduce_fusion
  59.8 5.1 %all-gather = bf16[4,1,128]{2,1,0:T(2,128)(2,1)S(1)} all-gather(bf16[1,1,128]{2,1,0:T(2,128)(2,1)S(1)} %bitcast.36), channel_id=1, replica_groups=mesh['grp'=2,'sp'=4,'tp'=4] {'tp'}, dimensions={0}, use_global_device_ids=true | all-gather | bytes 1280 | tf_op jit(solution)/shard_map/all_gather | solution.py:114
  64.9 0.1 fusion.16
  65.0 7.3 %all_gather.17 = bf16[128,2048]{0,1:T(8,128)(2,1)S(1)} all-gather(bf16[128,512]{0,1:T(8,128)(2,1)S(1)} %fusion.16), channel_id=1, replica_groups=mesh['grp'=2,'sp'=4,'tp'=4] {'tp'}, dimensions={1}, use_global_device_ids=true | all-gather | bytes 655360 | tf_op jit(solution)/shard_map/all_gather | solution.py:113
  72.3 21.2 %all-gather.3.cloned.1.call-done = bf16[2048,1024]{1,0:T(8,128)(2,1)} async-done(((bf16[512,1024]{1,0:T(8,128)(2,1)}), bf16[2048,1024]{1,0:T(8,128)(2,1)}) %all-gather.3.cloned.1.call-update) | async-done | bytes 4194320 | tf_op jit(solution)/shard_map/all_gather | solution.py:121
  93.5 3.6 %fusion.3 = bf16[128,1024]{1,0:T(8,128)(2,1)} fusion(bf16[128,2048]{0,1:T(8,128)(2,1)S(1)} %all_gather.17, bf16[2048,1024]{1,0:T(8,128)(2,1)} %all-gather.3.cloned.1.call-done, f32[128]{0:T(128)S(1)} %add_rsqrt_fusion), kind=kOutput, calls=%fused_computation.8 | convolution fusion | flops 537133056 | bytes 4981248 | tf_op jit(solution)/shard_map/dot_general | solution.py:119
  (17 shorter events, 0.1 us)
Async XLA Ops:
  6.5 1.8 %copy-start = (bf16[768,768]{1,0:T(8,128)(2,1)S(1)}, bf16[768,768]{1,0:T(8,128)(2,1)}, u32[]{:S(2)}) copy-start(bf16[768,768]{1,0:T(8,128)(2,1)} %param.15) | copy-start | bytes 3538948
  6.5 51.5 %copy-start.1 = (bf16[256,512]{1,0:T(8,128)(2,1)S(1)}, bf16[256,512]{1,0:T(8,128)(2,1)}, u32[]{:S(2)}) copy-start(bf16[256,512]{1,0:T(8,128)(2,1)} %param.16) | copy-start | bytes 786436
  6.5 86.9 %all-gather.3.cloned.1.call-start = ((), (), s32[]{:S(2)}) async-start(), calls=%async_computation | async-start | bytes 5242880 | tf_op jit(solution)/shard_map/all_gather | solution.py:121
  58.4 6.5 %copy-start.2 = (f32[512]{0:T(512)S(1)}, f32[512]{0:T(512)}, u32[]{:S(2)}) copy-start(f32[512]{0:T(512)} %param.18) | copy-start | bytes 6148
Sparse Core Ops, SparseCore 0:
  8.9 84.5 all-gather.2
where the time goes:
time: 104 us
  blocking collectives  56.7 us (55%)
  waiting for transfers between devices  21.9 us (21%)
  between operations  13.5 us (13%)
  matrix products  6.45 us (6%)
  other arithmetic  4.14 us (4%)
  local copies, waits for them, and re-layouts  1.25 us (1%)
    all_gather x1, blocking collectives, on_device(): turned_keys = lax.all_gather(key_turned, ('sp', 'tp'), axis=0, tiled=True)  24.3 us
    all_gather x1, waiting for transfers between devices, on_device(): lax.all_gather(out_weight, 'sp', axis=0, tiled=True)  21.2 us
    all_gather x1, blocking collectives, on_device(): latents = lax.all_gather(latent_normed, ('sp', 'tp'), axis=0, tiled=True)  20 us
    all_gather x1, blocking collectives, on_device(): lax.all_gather(gained, 'tp', axis=1, tiled=True)  7.27 us
    all_gather x1, blocking collectives, on_device(): lax.all_gather(square_part[:, None].astype(jnp.bfloat16), 'tp', axis=1, t...  5.06 us
    dot_general x1, matrix products, on_device(): jnp.dot(all_gained, lax.all_gather(out_weight, 'sp', axis=0, tiled=True),...  3.64 us
  transfers between devices with their start and end apart: 1, of which 1 were waited for; matrix products, arithmetic and copies ran while one was open for 8% of the time, Pallas kernels for 0%

commit v1 on v0

--- a/solution.py
+++ b/solution.py
@@ -1,6 +1,11 @@
+import functools
+
 import jax
 import jax.numpy as jnp
+import numpy as np
 from jax import lax
+from jax.experimental import pallas as pl
+from jax.experimental.pallas import tpu as pltpu
 from jax.sharding import PartitionSpec as P
 
 HEADS = 16
@@ -125,6 +130,352 @@
     return (own_sums * lax.rsqrt(mean_square + norm_eps)[:, None]).astype(jnp.bfloat16)
 
 
+CHUNKS = 4
+MOST_STEPS = 8
+
+
+def rope_table(tokens, width):
+    half = width // 2
+    inverse = np.float32(rope_theta) ** (-np.arange(half, dtype=np.float32) / np.float32(half))
+    angles = np.arange(tokens, dtype=np.float32)[:, None] * inverse.astype(np.float32)[None, :]
+    wide = angles.astype(np.float32).astype(np.float64)
+    cosine, sine = np.cos(wide), np.sin(wide)
+    return np.concatenate([cosine, cosine, -sine, sine], axis=1).astype(np.float32)
+
+
+def turned(wide, table):
+    width = wide.shape[-1]
+    half = width // 2
+    swapped = jnp.concatenate([wide[:, half:], wide[:, :half]], axis=1)
+    return wide * table[:, :width] + swapped * table[:, width:]
+
+
+def kernel(
+    n_sp, n_tp,
+    ql, kl, rk, qg, lg, og, table, qup, kup, vup, ow, out,
+    lat, rot, wbuf, qbuf, kbuf, vbuf, latn, kturn, qfull, qnorm, gall, acc,
+    local, s1_send, s1_recv, s2_send, s2_recv, g_send, g_recv,
+    w_send, w_recv, y_send, y_recv,
+):
+    z, t, g = lax.axis_index("sp"), lax.axis_index("tp"), lax.axis_index("grp")
+    parity = lax.rem(g, 2)
+    partner = g + 1 - 2 * parity
+    block_rows = ql.shape[0]
+    depth = ow.shape[0]
+    half = depth // 2
+    piece = half // CHUNKS
+    heads = kup.shape[1] // NOPE_DIM
+    cols = heads * VALUE_DIM
+    head_width = NOPE_DIM + ROPE_DIM
+    keys = n_sp * n_tp * kl.shape[0]
+
+    near = pl.ds(pl.multiple_of(parity * half, half), half)
+    far = pl.ds(pl.multiple_of((1 - parity) * half, half), half)
+    loads = [
+        pltpu.make_async_copy(ow.at[near], wbuf.at[z, near], local.at[0]),
+        pltpu.make_async_copy(kl, lat.at[z, t], local.at[1]),
+        pltpu.make_async_copy(rk, rot.at[z, t], local.at[2]),
+        pltpu.make_async_copy(qup, qbuf, local.at[3]),
+        pltpu.make_async_copy(kup, kbuf, local.at[4]),
+        pltpu.make_async_copy(vup, vbuf, local.at[5]),
+        pltpu.make_async_copy(ow.at[far], wbuf.at[z, far], local.at[6]),
+    ]
+    for load in loads:
+        load.start()
+
+    barrier = pltpu.get_barrier_semaphore()
+    for d in range(1, n_sp):
+        pl.semaphore_signal(barrier, inc=1, device_id={"sp": lax.rem(z + d, n_sp)}, device_id_type=MESH)
+    for d in range(1, n_tp):
+        pl.semaphore_signal(barrier, inc=1, device_id={"tp": lax.rem(t + d, n_tp)}, device_id_type=MESH)
+    pl.semaphore_signal(barrier, inc=1, device_id={"grp": partner}, device_id_type=MESH)
+    pl.semaphore_wait(barrier, n_sp + n_tp - 1)
+
+    def remote(src, dst, send, recv, target):
+        return pltpu.make_async_remote_copy(
+            src_ref=src, dst_ref=dst, send_sem=send, recv_sem=recv,
+            device_id=target, device_id_type=MESH,
+        )
+
+    first = []
+    for d in range(1, n_sp):
+        target = {"sp": lax.rem(z + d, n_sp)}
+        first.append(remote(kl, lat.at[z, t], s1_send.at[0, d], s1_recv.at[0, d], target))
+        first.append(remote(rk, rot.at[z, t], s1_send.at[1, d], s1_recv.at[1, d], target))
+    for copy in first:
+        copy.start()
+
+    def rows_of(b, c):
+        return wbuf.at[b, pl.ds(pl.multiple_of(parity * half + c * piece, piece), piece)]
+
+    def far_rows_of(b, c):
+        return wbuf.at[b, pl.ds(pl.multiple_of((1 - parity) * half + c * piece, piece), piece)]
+
+    def along(b, c, up):
+        return remote(
+            rows_of(b, c), rows_of(b, c), w_send.at[up, b, c], w_recv.at[b, c],
+            {"sp": z + 1 if up else z - 1},
+        )
+
+    def across(b, c):
+        return remote(rows_of(b, c), rows_of(b, c), y_send.at[b, c], y_recv.at[b, c], {"grp": partner})
+
+    has_up, has_down = z < n_sp - 1, z > 0
+    loads[0].wait()
+    for c in range(CHUNKS):
+        @pl.when(has_up)
+        def _():
+            along(z, c, 1).start()
+
+        @pl.when(has_down)
+        def _():
+            along(z, c, 0).start()
+
+    def event(k, c):
+        @pl.when(z >= k)
+        def _():
+            b = z - k
+            along(b, c, 1).wait_recv()
+
+            @pl.when(has_up)
+            def _():
+                along(b, c, 1).start()
+
+            across(b, c).start()
+
+        @pl.when(z + k < n_sp)
+        def _():
+            b = z + k
+            along(b, c, 0).wait_recv()
+
+            @pl.when(has_down)
+            def _():
+                along(b, c, 0).start()
+
+            across(b, c).start()
+
+    def block_product(b):
+        acc[...] += jnp.dot(gall[b, :, :cols], wbuf[b], preferred_element_type=jnp.float32)
+
+    def finish(k):
+        @pl.when(z >= k)
+        def _():
+            for c in range(CHUNKS):
+                across(z - k, c).wait_recv()
+            block_product(z - k)
+
+        @pl.when(z + k < n_sp)
+        def _():
+            for c in range(CHUNKS):
+                across(z + k, c).wait_recv()
+            block_product(z + k)
+
+    second = []
+    for d in range(1, n_tp):
+        target = {"tp": lax.rem(t + d, n_tp)}
+        second.append(remote(lat.at[:, t], lat.at[:, t], s2_send.at[0, d], s2_recv.at[0, d], target))
+        second.append(remote(rot.at[:, t], rot.at[:, t], s2_send.at[1, d], s2_recv.at[1, d], target))
+
+    def queries():
+        wide = ql[...].astype(jnp.float32)
+        mean = jnp.mean(wide * wide, axis=-1, keepdims=True)
+        qnorm[...] = (wide * lax.rsqrt(mean + norm_eps) * qg[...]).astype(jnp.bfloat16)
+        loads[3].wait()
+        qfull[...] = jnp.dot(qnorm[...], qbuf[...], preferred_element_type=jnp.float32).astype(
+            jnp.bfloat16
+        )
+
+    def spread():
+        loads[1].wait()
+        loads[2].wait()
+        for copy in first:
+            copy.wait_recv()
+        for copy in second:
+            copy.start()
+
+    def latents():
+        for copy in second:
+            copy.wait_recv()
+        wide = lat[...].reshape(keys, lat.shape[-1]).astype(jnp.float32)
+        mean = jnp.mean(wide * wide, axis=-1, keepdims=True)
+        latn[...] = (wide * lax.rsqrt(mean + norm_eps) * lg[...]).astype(jnp.bfloat16)
+        spun = rot[...].reshape(keys, rot.shape[-1]).astype(jnp.float32)
+        kturn[...] = turned(spun, table[...]).astype(jnp.bfloat16)
+        loads[4].wait()
+        loads[5].wait()
+
+    transposed = (((1,), (1,)), ((), ()))
+
+    def attend(h):
+        start = h * head_width
+        plain = qfull[:, start : start + NOPE_DIM]
+        spun = qfull[:, start + NOPE_DIM : start + head_width].astype(jnp.float32)
+        own = table[pl.ds(pl.multiple_of(z * block_rows, block_rows), block_rows), :]
+        spun = turned(spun, own).astype(jnp.bfloat16)
+        key_plain = jnp.dot(
+            latn[...], kbuf[:, h * NOPE_DIM : (h + 1) * NOPE_DIM], preferred_element_type=jnp.float32
+        ).astype(jnp.bfloat16)
+        scores = lax.dot_general(plain, key_plain, transposed, preferred_element_type=jnp.float32)
+        scores = scores + lax.dot_general(
+            spun, kturn[...], transposed, preferred_element_type=jnp.float32
+        )
+        scores = scores * (head_width ** (-0.5))
+        expo = jnp.exp(scores - jnp.max(scores, axis=-1, keepdims=True))
+        total = jnp.sum(expo, axis=-1, keepdims=True)
+        mix = jnp.dot(expo.astype(jnp.bfloat16), latn[...], preferred_element_type=jnp.float32)
+        mix = (mix / total).astype(jnp.bfloat16)
+        head_out = jnp.dot(
+            mix, vbuf[:, h * VALUE_DIM : (h + 1) * VALUE_DIM], preferred_element_type=jnp.float32
+        ).astype(jnp.bfloat16)
+        wide = head_out.astype(jnp.float32)
+        gained = wide * og[:, h * VALUE_DIM : (h + 1) * VALUE_DIM]
+        gall[t, :, h * VALUE_DIM : (h + 1) * VALUE_DIM] = gained.astype(jnp.bfloat16)
+        square = jnp.sum(wide * wide, axis=-1, keepdims=True)
+        if h:
+            square = square + acc[:, :1]
+        acc[:, :VALUE_DIM] = jnp.broadcast_to(square, (block_rows, VALUE_DIM))
+        if h == heads - 1:
+            gall[t, :, cols:] = acc[:, :VALUE_DIM].astype(jnp.bfloat16)
+
+    shares = [
+        remote(gall.at[t], gall.at[t], g_send.at[d], g_recv.at[d], {"tp": lax.rem(t + d, n_tp)})
+        for d in range(1, n_tp)
+    ]
+
+    def share():
+        for copy in shares:
+            copy.start()
+
+    def own_product():
+        for copy in shares:
+            copy.wait_recv()
+        loads[6].wait()
+        acc[...] = jnp.zeros_like(acc)
+        block_product(z)
+
+    attends = [functools.partial(attend, h) for h in range(heads)]
+    split = (heads + 1) // 2
+    tasks = {
+        0: [queries, spread],
+        1: [latents] + attends[:1],
+        2: attends[1 : split + 1],
+        3: attends[split + 1 :],
+        4: [share],
+        5: [],
+        6: [own_product],
+    }
+    slot = 0
+    for k in range(1, n_sp):
+        for c in range(CHUNKS):
+            for task in tasks.pop(slot, []):
+                task()
+            event(k, c)
+            slot += 1
+        if k > 2:
+            finish(k - 2)
+    for left in sorted(tasks):
+        for task in tasks[left]:
+            task()
+    for k in range(max(n_sp - 2, 1), n_sp):
+        finish(k)
+
+    squares = gall[0, :, cols : cols + 1].astype(jnp.float32)
+    for p in range(1, n_tp):
+        squares = squares + gall[p, :, cols : cols + 1].astype(jnp.float32)
+    scale = lax.rsqrt(squares / (n_tp * cols) + norm_eps)
+    out[...] = (acc[...] * scale).astype(out.dtype)
+
+    for copy in first + second + shares:
+        copy.wait_send()
+    for c in range(CHUNKS):
+        @pl.when(has_up)
+        def _():
+            along(z, c, 1).wait_send()
+
+        @pl.when(has_down)
+        def _():
+            along(z, c, 0).wait_send()
+
+    for k in range(1, n_sp):
+        for c in range(CHUNKS):
+            @pl.when(z >= k)
+            def _():
+                across(z - k, c).wait_send()
+
+            @pl.when(jnp.logical_and(z >= k, has_up))
+            def _():
+                along(z - k, c, 1).wait_send()
+
+            @pl.when(z + k < n_sp)
+            def _():
+                across(z + k, c).wait_send()
+
+            @pl.when(jnp.logical_and(z + k < n_sp, has_down))
+            def _():
+                along(z + k, c, 0).wait_send()
+
+
+MESH = pl.DeviceIdType.MESH
+
+
+def on_device_fused(
+    n_sp, n_tp,
+    query_latent, key_latent, rotary_key, query_gain, latent_gain,
+    query_up, key_up, value_up, out_gain, out_weight,
+):
+    block_rows, row_count = query_latent.shape[0], key_latent.shape[0]
+    rank, width = key_latent.shape[1], rotary_key.shape[1]
+    keys = n_sp * n_tp * row_count
+    depth, features = out_weight.shape
+    cols = value_up.shape[1]
+    vmem, bf16, dma = pltpu.VMEM, jnp.bfloat16, pltpu.SemaphoreType.DMA
+    table = jnp.asarray(rope_table(keys, width))
+    in_vmem = pl.BlockSpec(memory_space=pltpu.VMEM)
+    in_hbm = pl.BlockSpec(memory_space=pl.ANY)
+    return pl.pallas_call(
+        functools.partial(kernel, n_sp, n_tp),
+        out_shape=jax.ShapeDtypeStruct((block_rows, features), bf16),
+        in_specs=[in_vmem] * 7 + [in_hbm] * 4,
+        out_specs=in_vmem,
+        scratch_shapes=[
+            vmem((n_sp, n_tp, row_count, rank), bf16),
+            vmem((n_sp, n_tp, row_count, width), bf16),
+            vmem((n_sp, depth, features), bf16),
+            vmem(query_up.shape, bf16),
+            vmem(key_up.shape, bf16),
+            vmem(value_up.shape, bf16),
+            vmem((keys, rank), bf16),
+            vmem((keys, width), bf16),
+            vmem((block_rows, query_up.shape[1]), bf16),
+            vmem(query_latent.shape, bf16),
+            vmem((n_tp, block_rows, cols + VALUE_DIM), bf16),
+            vmem((block_rows, features), jnp.float32),
+            dma((7,)),
+            dma((2, n_sp)),
+            dma((2, n_sp)),
+            dma((2, n_tp)),
+            dma((2, n_tp)),
+            dma((n_tp,)),
+            dma((n_tp,)),
+            dma((2, n_sp, CHUNKS)),
+            dma((n_sp, CHUNKS)),
+            dma((n_sp, CHUNKS)),
+            dma((n_sp, CHUNKS)),
+        ],
+        compiler_params=pltpu.CompilerParams(
+            collective_id=0, has_side_effects=True, vmem_limit_bytes=48 * 1024 * 1024
+        ),
+    )(
+        query_latent, key_latent, rotary_key, query_gain[None], latent_gain[None], out_gain[None],
+        table, query_up, key_up, value_up, out_weight,
+    )
+
+
+def fits_fused(mesh):
+    n_grp, n_sp, n_tp = (mesh.shape[name] for name in ("grp", "sp", "tp"))
+    return n_grp % 2 == 0 and 1 < n_sp <= MOST_STEPS and n_sp == n_tp
+
+
 def solution(mesh):
     in_specs = (
         P(("grp", "sp"), None),
@@ -139,6 +490,9 @@
         P("sp", "tp"),
     )
     out_specs = P(("grp", "sp"), "tp")
+    step = on_device
+    if fits_fused(mesh):
+        step = functools.partial(on_device_fused, mesh.shape["sp"], mesh.shape["tp"])
     return jax.shard_map(
-        on_device, mesh=mesh, in_specs=in_specs, out_specs=out_specs, check_vma=False
-    )
+        step, mesh=mesh, in_specs=in_specs, out_specs=out_specs, check_vma=False
+    )

time: 104 us -> 61 us (0.59)
  blocking collectives: 56.7 us -> 0 us
  Pallas kernels: 0 us -> 50 us
  waiting for transfers between devices: 21.9 us -> 0 us
  between operations: 13.5 us -> 0.02 us
  local copies, waits for them, and re-layouts: 1.25 us -> 10.4 us
  matrix products: 6.45 us -> 0 us
  other arithmetic: 4.14 us -> 0 us
    all_gather x4 -> x0, blocking collectives: 56.7 us -> none  [the longest x1 24.3 us: on_device(): turned_keys = lax.all_gather(key_turned, ('sp', 'tp'), axis=0, tiled=True)]
    pallas_call x0 -> x1, Pallas kernels: none -> 50 us  [on_device_fused(): pl.pallas_call(functools.partial(kernel, n_sp, n_tp), out_shape=jax.Shape...]
    all_gather x1 -> x0, waiting for transfers between devices: 21.2 us -> none  [on_device(): lax.all_gather(out_weight, 'sp', axis=0, tiled=True)]
    unnamed x6 -> x21, local copies, waits for them, and re-layouts: 0.01 us -> 9.75 us
    dot_general x6 -> x0, matrix products: 6.45 us -> none  [the longest x1 3.64 us: on_device(): jnp.dot(all_gained, lax.all_gather(out_weight, 'sp', axis=0, tiled=True),...]
    reduce_sum x4 -> x0, other arithmetic: 2.06 us -> none  [the longest x2 1.88 us: rms_scaled(): jnp.mean(widened * widened, axis=-1, keepdims=True) + norm_eps]
    convert_element_type x6 -> x0, other arithmetic: 1.66 us -> none  [the longest x1 0.8 us: on_device(): latent_normed = rms_scaled(key_latent, latent_gain).astype(jnp.bfloat16)]
    reshape x1 -> x0, local copies, waits for them, and re-layouts: 1.08 us -> none  [on_device(): value_heads = value_up.reshape(KVRANK, head_local, VALUE_DIM)]
  transfers between devices with their start and end apart: 1 -> 0, of which waited for: 1 -> 0; matrix products, arithmetic and copies ran while one was open for 8% -> 0% of each run, Pallas kernels for 0% -> 0%
where the time goes in v1:
time: 61 us; the launch traced here: 60.5 us
  Pallas kernels  50 us (82%)
  local copies, waits for them, and re-layouts  10.4 us (17%)
    pallas_call x1, Pallas kernels, on_device_fused(): pl.pallas_call(functools.partial(kernel, n_sp, n_tp), out_shape=jax.Shape...  50 us
    unnamed x21, local copies, waits for them, and re-layouts  9.75 us

profile of v1, /device:TPU:0, one launch (start us, length us, event | category | flops | bytes accessed | tf_op | source)
XLA Modules:
  0.0 60.5 jit_solution(1561732468424288701)
XLA Ops:
  0.0 0.7 %broadcast_in_dim.9.qg = f32[1,768]{1,0:T(1,128)S(1)} reshape(f32[768]{0:T(1024)} %param.14) | data formatting | bytes 6144 | tf_op jit(solution)/shard_map/broadcast_in_dim | solution.py:469
  0.7 0.0 copy-start
  0.7 1.3 %copy-done = bf16[768,768]{1,0:T(8,128)(2,1)S(1)} copy-done((bf16[768,768]{1,0:T(8,128)(2,1)S(1)}, bf16[768,768]{1,0:T(8,128)(2,1)}, u32[]{:S(2)}) %copy-start) | copy-done | bytes 1179672
  2.0 0.0 copy-start.1
  2.0 1.2 %copy-done.1 = bf16[512,1024]{1,0:T(8,128)(2,1)S(1)} copy-done((bf16[512,1024]{1,0:T(8,128)(2,1)S(1)}, bf16[512,1024]{1,0:T(8,128)(2,1)}, u32[]{:S(2)}) %copy-start.1) | copy-done | bytes 1048600
  3.2 0.0 copy-start.2
  3.2 0.9 %copy-done.2 = bf16[256,512]{1,0:T(8,128)(2,1)S(1)} copy-done((bf16[256,512]{1,0:T(8,128)(2,1)S(1)}, bf16[256,512]{1,0:T(8,128)(2,1)}, u32[]{:S(2)}) %copy-start.2) | copy-done | bytes 262168
  4.1 0.0 copy-start.3
  4.1 0.9 %copy-done.3 = bf16[256,512]{1,0:T(8,128)(2,1)S(1)} copy-done((bf16[256,512]{1,0:T(8,128)(2,1)S(1)}, bf16[256,512]{1,0:T(8,128)(2,1)}, u32[]{:S(2)}) %copy-start.3) | copy-done | bytes 262168
  5.1 0.0 copy-start.4
  5.1 0.9 %copy-done.4 = f32[512,128]{1,0:T(8,128)S(1)} copy-done((f32[512,128]{1,0:T(8,128)S(1)}, f32[512,128]{1,0:T(8,128)}, u32[]{:S(2)}) %copy-start.4) | copy-done | bytes 262168
  6.0 0.0 copy-start.5
  6.0 0.9 %copy-done.5 = bf16[128,768]{1,0:T(8,128)(2,1)S(1)} copy-done((bf16[128,768]{1,0:T(8,128)(2,1)S(1)}, bf16[128,768]{1,0:T(8,128)(2,1)}, u32[]{:S(2)}) %copy-start.5) | copy-done | bytes 196632
  7.0 0.0 copy-start.6
  7.0 0.7 %copy-done.6 = bf16[32,256]{1,0:T(8,128)(2,1)S(1)} copy-done((bf16[32,256]{1,0:T(8,128)(2,1)S(1)}, bf16[32,256]{1,0:T(8,128)(2,1)}, u32[]{:S(2)}) %copy-start.6) | copy-done | bytes 16408
  7.7 0.0 copy-start.7
  7.7 0.7 %copy-done.7 = bf16[32,64]{1,0:T(8,128)(2,1)S(1)} copy-done((bf16[32,64]{1,0:T(8,128)(2,1)S(1)}, bf16[32,64]{1,0:T(8,128)(2,1)}, u32[]{:S(2)}) %copy-start.7) | copy-done | bytes 4120
  8.4 0.0 copy-start.8
  8.4 0.7 %copy-done.8 = f32[512]{0:T(512)S(1)} copy-done((f32[512]{0:T(512)S(1)}, f32[512]{0:T(512)}, u32[]{:S(2)}) %copy-start.8) | copy-done | bytes 2072
  9.1 0.0 copy-start.9
  9.1 0.7 %copy-done.9 = f32[256]{0:T(256)S(1)} copy-done((f32[256]{0:T(256)S(1)}, f32[256]{0:T(256)}, u32[]{:S(2)}) %copy-start.9) | copy-done | bytes 1048
  9.7 50.0 %shard_map.109 = bf16[128,1024]{1,0:T(8,128)(2,1)S(1)} custom-call(bf16[128,768]{1,0:T(8,128)(2,1)S(1)} %copy-done.5, bf16[32,256]{1,0:T(8,128)(2,1)S(1)} %copy-done.6, bf16[32,64]{1,0:T(8,128)(2,1)S(1)} %copy-done.7, f32[1,768]{1,0:T(1,128)S(1)} %broadcast_in_dim.9.qg, f32[1,256]{1,0:T(1,128)S(1)} %bitcast.3, f32[1,512]{1,0:T(1,128)S(1)} %bitcast.2, ...), custom_call_target="tpu_custom_call" | custom-call | tf_op jit(solution)/shard_map/pallas_call | solution.py:435
  59.8 0.7 %copy.13 = bf16[128,1024]{1,0:T(8,128)(2,1)} copy(bf16[128,1024]{1,0:T(8,128)(2,1)S(1)} %shard_map.109) | data formatting | bytes 524288
Async XLA Ops:
  0.7 1.3 %copy-start = (bf16[768,768]{1,0:T(8,128)(2,1)S(1)}, bf16[768,768]{1,0:T(8,128)(2,1)}, u32[]{:S(2)}) copy-start(bf16[768,768]{1,0:T(8,128)(2,1)} %qup.1) | copy-start | bytes 3538948
  2.0 1.2 %copy-start.1 = (bf16[512,1024]{1,0:T(8,128)(2,1)S(1)}, bf16[512,1024]{1,0:T(8,128)(2,1)}, u32[]{:S(2)}) copy-start(bf16[512,1024]{1,0:T(8,128)(2,1)} %ow.1) | copy-start | bytes 3145732
  3.2 0.9 %copy-start.2 = (bf16[256,512]{1,0:T(8,128)(2,1)S(1)}, bf16[256,512]{1,0:T(8,128)(2,1)}, u32[]{:S(2)}) copy-start(bf16[256,512]{1,0:T(8,128)(2,1)} %kup.1) | copy-start | bytes 786436
  4.1 0.9 %copy-start.3 = (bf16[256,512]{1,0:T(8,128)(2,1)S(1)}, bf16[256,512]{1,0:T(8,128)(2,1)}, u32[]{:S(2)}) copy-start(bf16[256,512]{1,0:T(8,128)(2,1)} %vup.1) | copy-start | bytes 786436
  5.1 0.9 %copy-start.4 = (f32[512,128]{1,0:T(8,128)S(1)}, f32[512,128]{1,0:T(8,128)}, u32[]{:S(2)}) copy-start(f32[512,128]{1,0:T(8,128)} %constant.2.clone.table) | copy-start | bytes 786436
  6.0 0.9 %copy-start.5 = (bf16[128,768]{1,0:T(8,128)(2,1)S(1)}, bf16[128,768]{1,0:T(8,128)(2,1)}, u32[]{:S(2)}) copy-start(bf16[128,768]{1,0:T(8,128)(2,1)} %ql.1) | copy-start | bytes 589828
  7.0 0.7 %copy-start.6 = (bf16[32,256]{1,0:T(8,128)(2,1)S(1)}, bf16[32,256]{1,0:T(8,128)(2,1)}, u32[]{:S(2)}) copy-start(bf16[32,256]{1,0:T(8,128)(2,1)} %kl.1) | copy-start | bytes 49156
  7.7 0.7 %copy-start.7 = (bf16[32,64]{1,0:T(8,128)(2,1)S(1)}, bf16[32,64]{1,0:T(8,128)(2,1)}, u32[]{:S(2)}) copy-start(bf16[32,64]{1,0:T(8,128)(2,1)} %rk.1) | copy-start | bytes 12292
  8.4 0.7 %copy-start.8 = (f32[512]{0:T(512)S(1)}, f32[512]{0:T(512)}, u32[]{:S(2)}) copy-start(f32[512]{0:T(512)} %param.19) | copy-start | bytes 6148
  9.1 0.7 %copy-start.9 = (f32[256]{0:T(256)S(1)}, f32[256]{0:T(256)}, u32[]{:S(2)}) copy-start(f32[256]{0:T(256)} %param.15) | copy-start | bytes 3076

commit v2 on v1

--- a/solution.py
+++ b/solution.py
@@ -131,6 +131,7 @@
 
 
 CHUNKS = 4
+LANES = 128
 MOST_STEPS = 8
 
 
@@ -152,10 +153,12 @@
 
 def kernel(
     n_sp, n_tp,
-    ql, kl, rk, qg, lg, og, table, qup, kup, vup, ow, out,
+    ql_hbm, kl, rk, qg_hbm, lg_hbm, og_hbm, table_hbm, qup, kup, vup, ow, out,
+    ql, qg, lg, og, table,
     lat, rot, wbuf, qbuf, kbuf, vbuf, latn, kturn, qfull, qnorm, gall, acc,
+    far_gained, far_out, far_in,
     local, s1_send, s1_recv, s2_send, s2_recv, g_send, g_recv,
-    w_send, w_recv, y_send, y_recv,
+    w_send, w_recv, y_send, y_recv, f_send, f_recv,
 ):
     z, t, g = lax.axis_index("sp"), lax.axis_index("tp"), lax.axis_index("grp")
     parity = lax.rem(g, 2)
@@ -170,15 +173,23 @@
     keys = n_sp * n_tp * kl.shape[0]
 
     near = pl.ds(pl.multiple_of(parity * half, half), half)
-    far = pl.ds(pl.multiple_of((1 - parity) * half, half), half)
+    far_half = pl.ds(pl.multiple_of((1 - parity) * half, half), half)
     loads = [
-        pltpu.make_async_copy(ow.at[near], wbuf.at[z, near], local.at[0]),
-        pltpu.make_async_copy(kl, lat.at[z, t], local.at[1]),
-        pltpu.make_async_copy(rk, rot.at[z, t], local.at[2]),
-        pltpu.make_async_copy(qup, qbuf, local.at[3]),
-        pltpu.make_async_copy(kup, kbuf, local.at[4]),
-        pltpu.make_async_copy(vup, vbuf, local.at[5]),
-        pltpu.make_async_copy(ow.at[far], wbuf.at[z, far], local.at[6]),
+        pltpu.make_async_copy(src, dst, local.at[i])
+        for i, (src, dst) in enumerate((
+            (kl, lat.at[z, t]),
+            (rk, rot.at[z, t]),
+            (ow.at[near], wbuf.at[z, near]),
+            (ql_hbm, ql),
+            (qg_hbm, qg),
+            (qup, qbuf),
+            (lg_hbm, lg),
+            (table_hbm, table),
+            (kup, kbuf),
+            (vup, vbuf),
+            (og_hbm, og),
+            (ow.at[far_half], wbuf.at[z, far_half]),
+        ))
     ]
     for load in loads:
         load.start()
@@ -200,16 +211,15 @@
     first = []
     for d in range(1, n_sp):
         target = {"sp": lax.rem(z + d, n_sp)}
-        first.append(remote(kl, lat.at[z, t], s1_send.at[0, d], s1_recv.at[0, d], target))
-        first.append(remote(rk, rot.at[z, t], s1_send.at[1, d], s1_recv.at[1, d], target))
+        first.append(remote(lat.at[z, t], lat.at[z, t], s1_send.at[0, d], s1_recv.at[0, d], target))
+        first.append(remote(rot.at[z, t], rot.at[z, t], s1_send.at[1, d], s1_recv.at[1, d], target))
+    loads[0].wait()
+    loads[1].wait()
     for copy in first:
         copy.start()
 
     def rows_of(b, c):
         return wbuf.at[b, pl.ds(pl.multiple_of(parity * half + c * piece, piece), piece)]
-
-    def far_rows_of(b, c):
-        return wbuf.at[b, pl.ds(pl.multiple_of((1 - parity) * half + c * piece, piece), piece)]
 
     def along(b, c, up):
         return remote(
@@ -221,7 +231,12 @@
         return remote(rows_of(b, c), rows_of(b, c), y_send.at[b, c], y_recv.at[b, c], {"grp": partner})
 
     has_up, has_down = z < n_sp - 1, z > 0
-    loads[0].wait()
+    reach = n_sp - 2
+    at_edge = jnp.logical_or(z == 0, z == n_sp - 1)
+    far = jnp.where(z == 0, n_sp - 1, 0)
+    ask = remote(gall.at[far, :, pl.ds(0, cols)], far_gained, f_send.at[0], f_recv.at[0], {"sp": far})
+    answer = remote(far_out, far_in, f_send.at[1], f_recv.at[1], {"sp": far})
+    loads[2].wait()
     for c in range(CHUNKS):
         @pl.when(has_up)
         def _():
@@ -237,9 +252,10 @@
             b = z - k
             along(b, c, 1).wait_recv()
 
-            @pl.when(has_up)
-            def _():
-                along(b, c, 1).start()
+            if k < reach:
+                @pl.when(has_up)
+                def _():
+                    along(b, c, 1).start()
 
             across(b, c).start()
 
@@ -248,9 +264,10 @@
             b = z + k
             along(b, c, 0).wait_recv()
 
-            @pl.when(has_down)
-            def _():
-                along(b, c, 0).start()
+            if k < reach:
+                @pl.when(has_down)
+                def _():
+                    along(b, c, 0).start()
 
             across(b, c).start()
 
@@ -277,23 +294,26 @@
         second.append(remote(rot.at[:, t], rot.at[:, t], s2_send.at[1, d], s2_recv.at[1, d], target))
 
     def queries():
+        loads[3].wait()
+        loads[4].wait()
+        loads[5].wait()
         wide = ql[...].astype(jnp.float32)
         mean = jnp.mean(wide * wide, axis=-1, keepdims=True)
-        qnorm[...] = (wide * lax.rsqrt(mean + norm_eps) * qg[...]).astype(jnp.bfloat16)
-        loads[3].wait()
+        gain = jnp.concatenate([qg[i : i + 1] for i in range(qg.shape[0])], axis=1)
+        qnorm[...] = (wide * lax.rsqrt(mean + norm_eps) * gain).astype(jnp.bfloat16)
         qfull[...] = jnp.dot(qnorm[...], qbuf[...], preferred_element_type=jnp.float32).astype(
             jnp.bfloat16
         )
 
     def spread():
-        loads[1].wait()
-        loads[2].wait()
         for copy in first:
             copy.wait_recv()
         for copy in second:
             copy.start()
 
     def latents():
+        for load in loads[6:11]:
+            load.wait()
         for copy in second:
             copy.wait_recv()
         wide = lat[...].reshape(keys, lat.shape[-1]).astype(jnp.float32)
@@ -301,8 +321,6 @@
         latn[...] = (wide * lax.rsqrt(mean + norm_eps) * lg[...]).astype(jnp.bfloat16)
         spun = rot[...].reshape(keys, rot.shape[-1]).astype(jnp.float32)
         kturn[...] = turned(spun, table[...]).astype(jnp.bfloat16)
-        loads[4].wait()
-        loads[5].wait()
 
     transposed = (((1,), (1,)), ((), ()))
 
@@ -337,47 +355,83 @@
         if h == heads - 1:
             gall[t, :, cols:] = acc[:, :VALUE_DIM].astype(jnp.bfloat16)
 
+    def head_part(h):
+        width = VALUE_DIM if h < heads - 1 else 2 * VALUE_DIM
+        return gall.at[t, :, pl.ds(h * VALUE_DIM, width)]
+
     shares = [
-        remote(gall.at[t], gall.at[t], g_send.at[d], g_recv.at[d], {"tp": lax.rem(t + d, n_tp)})
-        for d in range(1, n_tp)
+        [
+            remote(head_part(h), head_part(h), g_send.at[h, d], g_recv.at[h, d], {"tp": lax.rem(t + d, n_tp)})
+            for d in range(1, n_tp)
+        ]
+        for h in range(heads)
     ]
 
-    def share():
-        for copy in shares:
+    def share(h):
+        for copy in shares[h]:
             copy.start()
 
+    def far_ask():
+        for copy in sum(shares, []):
+            copy.wait_recv()
+
+        @pl.when(at_edge)
+        def _():
+            ask.start()
+
+    def far_product():
+        loads[11].wait()
+
+        @pl.when(at_edge)
+        def _():
+            ask.wait_recv()
+            far_out[...] = jnp.dot(
+                far_gained[...], wbuf[z], preferred_element_type=jnp.float32
+            ).astype(jnp.bfloat16)
+
     def own_product():
-        for copy in shares:
-            copy.wait_recv()
-        loads[6].wait()
         acc[...] = jnp.zeros_like(acc)
         block_product(z)
 
-    attends = [functools.partial(attend, h) for h in range(heads)]
-    split = (heads + 1) // 2
+    def far_answer():
+        @pl.when(at_edge)
+        def _():
+            answer.start()
+
+    work = [functools.partial(attend, h) for h in range(heads)]
+    sends = [functools.partial(share, h) for h in range(heads)]
+    middle = (heads + 1) // 2
+    early = [call for pair in zip(work[:middle], [None] + sends[: middle - 1]) for call in pair if call]
+    late = [
+        call
+        for pair in zip(work[middle:], sends[middle - 1 : heads - 1])
+        for call in pair
+    ]
     tasks = {
         0: [queries, spread],
-        1: [latents] + attends[:1],
-        2: attends[1 : split + 1],
-        3: attends[split + 1 :],
-        4: [share],
-        5: [],
-        6: [own_product],
+        1: [latents] + early,
+        2: late,
+        3: sends[heads - 1 :],
+        4: [far_ask],
+        6: [far_product, own_product, far_answer],
     }
     slot = 0
-    for k in range(1, n_sp):
+    for k in range(1, reach + 1):
         for c in range(CHUNKS):
             for task in tasks.pop(slot, []):
                 task()
             event(k, c)
             slot += 1
-        if k > 2:
-            finish(k - 2)
     for left in sorted(tasks):
         for task in tasks[left]:
             task()
-    for k in range(max(n_sp - 2, 1), n_sp):
+    for k in range(1, reach + 1):
         finish(k)
+
+    @pl.when(at_edge)
+    def _():
+        answer.wait_recv()
+        acc[...] += far_in[...].astype(jnp.float32)
 
     squares = gall[0, :, cols : cols + 1].astype(jnp.float32)
     for p in range(1, n_tp):
@@ -385,7 +439,7 @@
     scale = lax.rsqrt(squares / (n_tp * cols) + norm_eps)
     out[...] = (acc[...] * scale).astype(out.dtype)
 
-    for copy in first + second + shares:
+    for copy in first + second + sum(shares, []):
         copy.wait_send()
     for c in range(CHUNKS):
         @pl.when(has_up)
@@ -396,23 +450,29 @@
         def _():
             along(z, c, 0).wait_send()
 
-    for k in range(1, n_sp):
+    @pl.when(at_edge)
+    def _():
+        ask.wait_send()
+        answer.wait_send()
+
+    for k in range(1, reach + 1):
         for c in range(CHUNKS):
             @pl.when(z >= k)
             def _():
                 across(z - k, c).wait_send()
 
-            @pl.when(jnp.logical_and(z >= k, has_up))
-            def _():
-                along(z - k, c, 1).wait_send()
-
             @pl.when(z + k < n_sp)
             def _():
                 across(z + k, c).wait_send()
 
-            @pl.when(jnp.logical_and(z + k < n_sp, has_down))
-            def _():
-                along(z + k, c, 0).wait_send()
+            if k < reach:
+                @pl.when(jnp.logical_and(z >= k, has_up))
+                def _():
+                    along(z - k, c, 1).wait_send()
+
+                @pl.when(jnp.logical_and(z + k < n_sp, has_down))
+                def _():
+                    along(z + k, c, 0).wait_send()
 
 
 MESH = pl.DeviceIdType.MESH
@@ -435,9 +495,14 @@
     return pl.pallas_call(
         functools.partial(kernel, n_sp, n_tp),
         out_shape=jax.ShapeDtypeStruct((block_rows, features), bf16),
-        in_specs=[in_vmem] * 7 + [in_hbm] * 4,
+        in_specs=[in_hbm] * 11,
         out_specs=in_vmem,
         scratch_shapes=[
+            vmem(query_latent.shape, bf16),
+            vmem((query_gain.shape[0] // LANES, LANES), jnp.float32),
+            vmem((1, rank), jnp.float32),
+            vmem((1, cols), jnp.float32),
+            vmem(table.shape, jnp.float32),
             vmem((n_sp, n_tp, row_count, rank), bf16),
             vmem((n_sp, n_tp, row_count, width), bf16),
             vmem((n_sp, depth, features), bf16),
@@ -450,30 +515,35 @@
             vmem(query_latent.shape, bf16),
             vmem((n_tp, block_rows, cols + VALUE_DIM), bf16),
             vmem((block_rows, features), jnp.float32),
-            dma((7,)),
+            vmem((block_rows, cols), bf16),
+            vmem((block_rows, features), bf16),
+            vmem((block_rows, features), bf16),
+            dma((12,)),
             dma((2, n_sp)),
             dma((2, n_sp)),
             dma((2, n_tp)),
             dma((2, n_tp)),
-            dma((n_tp,)),
-            dma((n_tp,)),
+            dma((cols // VALUE_DIM, n_tp)),
+            dma((cols // VALUE_DIM, n_tp)),
             dma((2, n_sp, CHUNKS)),
             dma((n_sp, CHUNKS)),
             dma((n_sp, CHUNKS)),
             dma((n_sp, CHUNKS)),
+            dma((2,)),
+            dma((2,)),
         ],
         compiler_params=pltpu.CompilerParams(
-            collective_id=0, has_side_effects=True, vmem_limit_bytes=48 * 1024 * 1024
+            collective_id=0, has_side_effects=True
         ),
     )(
-        query_latent, key_latent, rotary_key, query_gain[None], latent_gain[None], out_gain[None],
+        query_latent, key_latent, rotary_key, query_gain.reshape(-1, LANES), latent_gain[None], out_gain[None],
         table, query_up, key_up, value_up, out_weight,
     )
 
 
 def fits_fused(mesh):
     n_grp, n_sp, n_tp = (mesh.shape[name] for name in ("grp", "sp", "tp"))
-    return n_grp % 2 == 0 and 1 < n_sp <= MOST_STEPS and n_sp == n_tp
+    return n_grp % 2 == 0 and 2 < n_sp <= MOST_STEPS and n_sp == n_tp
 
 
 def solution(mesh):

time: 61 us -> 48.5 us (0.80)
  the two profiles are of different devices: /device:TPU:0 before, /device:TPU:9 now
where the time goes in v2:
time: 48.5 us; the launch traced here: 48.4 us
  Pallas kernels  46.7 us (96%)
  local copies, waits for them, and re-layouts  1.67 us (3%)
    pallas_call x1, Pallas kernels, on_device_fused(): pl.pallas_call(functools.partial(kernel, n_sp, n_tp), out_shape=jax.Shape...  46.7 us
    unnamed x1, local copies, waits for them, and re-layouts  1.67 us

profile of v2, /device:TPU:9, one launch (start us, length us, event | category | flops | bytes accessed | tf_op | source)
XLA Modules:
  0.0 48.4 jit_solution(4231784487798164697)
XLA Ops:
  0.0 46.7 %shard_map.109 = bf16[128,1024]{1,0:T(8,128)(2,1)} custom-call(bf16[128,768]{1,0:T(8,128)(2,1)} %ql_hbm.1, bf16[32,256]{1,0:T(8,128)(2,1)} %kl.1, bf16[32,64]{1,0:T(8,128)(2,1)} %rk.1, f32[6,128]{1,0:T(8,128)} %bitcast.3, f32[1,256]{1,0:T(1,128)} %bitcast.5, f32[1,512]{1,0:T(1,128)} %bitcast.4, f32[512,128]{1,0:T(8,128)} %constant.2.clone.table_hbm, ...), custom_call_target="tpu_custom_call" | custom-call | tf_op jit(solution)/shard_map/pallas_call | solution.py:495
  46.7 1.7 %copy.13 = bf16[128,1024]{1,0:T(8,128)(2,1)} copy(bf16[128,1024]{1,0:T(8,128)(2,1)} %shard_map.109) | data formatting | bytes 524288

commit v3 on v2

--- a/solution.py
+++ b/solution.py
@@ -227,6 +227,15 @@
             {"sp": z + 1 if up else z - 1},
         )
 
+    def far_rows_of(b, c):
+        return wbuf.at[b, pl.ds(pl.multiple_of((1 - parity) * half + c * piece, piece), piece)]
+
+    def along_far(c):
+        return remote(
+            far_rows_of(z, c), far_rows_of(z, c), y_send.at[z, c], y_recv.at[z, c],
+            {"sp": jnp.where(z == 0, 1, n_sp - 2)},
+        )
+
     def across(b, c):
         return remote(rows_of(b, c), rows_of(b, c), y_send.at[b, c], y_recv.at[b, c], {"grp": partner})
 
@@ -257,7 +266,12 @@
                 def _():
                     along(b, c, 1).start()
 
-            across(b, c).start()
+            if k == 1:
+                @pl.when(z > 1)
+                def _():
+                    across(b, c).start()
+            else:
+                across(b, c).start()
 
         @pl.when(z + k < n_sp)
         def _():
@@ -269,7 +283,12 @@
                 def _():
                     along(b, c, 0).start()
 
-            across(b, c).start()
+            if k == 1:
+                @pl.when(z < n_sp - 2)
+                def _():
+                    across(b, c).start()
+            else:
+                across(b, c).start()
 
     def block_product(b):
         acc[...] += jnp.dot(gall[b, :, :cols], wbuf[b], preferred_element_type=jnp.float32)
@@ -304,6 +323,14 @@
         qfull[...] = jnp.dot(qnorm[...], qbuf[...], preferred_element_type=jnp.float32).astype(
             jnp.bfloat16
         )
+
+    def far_halves():
+        loads[11].wait()
+
+        @pl.when(at_edge)
+        def _():
+            for c in range(CHUNKS):
+                along_far(c).start()
 
     def spread():
         for copy in first:
@@ -380,8 +407,6 @@
             ask.start()
 
     def far_product():
-        loads[11].wait()
-
         @pl.when(at_edge)
         def _():
             ask.wait_recv()
@@ -408,12 +433,12 @@
         for call in pair
     ]
     tasks = {
-        0: [queries, spread],
+        0: [queries, far_halves, spread],
         1: [latents] + early,
         2: late,
         3: sends[heads - 1 :],
         4: [far_ask],
-        6: [far_product, own_product, far_answer],
+        7: [far_product, own_product, far_answer],
     }
     slot = 0
     for k in range(1, reach + 1):
@@ -454,14 +479,16 @@
     def _():
         ask.wait_send()
         answer.wait_send()
+        for c in range(CHUNKS):
+            along_far(c).wait_send()
 
     for k in range(1, reach + 1):
         for c in range(CHUNKS):
-            @pl.when(z >= k)
+            @pl.when(z >= max(k, 2))
             def _():
                 across(z - k, c).wait_send()
 
-            @pl.when(z + k < n_sp)
+            @pl.when(z + max(k, 2) < n_sp)
             def _():
                 across(z + k, c).wait_send()
 

time: 48.5 us -> 46.4 us (0.957)
  the two profiles are of different devices: /device:TPU:9 before, /device:TPU:0 now
where the time goes in v3:
time: 46.4 us; the launch traced here: 46.3 us
  Pallas kernels  44.6 us (96%)
  local copies, waits for them, and re-layouts  1.67 us (4%)
    pallas_call x1, Pallas kernels, on_device_fused(): pl.pallas_call(functools.partial(kernel, n_sp, n_tp), out_shape=jax.Shape...  44.6 us
    unnamed x1, local copies, waits for them, and re-layouts  1.67 us

profile of v3, /device:TPU:0, one launch (start us, length us, event | category | flops | bytes accessed | tf_op | source)
XLA Modules:
  0.0 46.3 jit_solution(7837935179437421656)
XLA Ops:
  0.0 44.6 %shard_map.109 = bf16[128,1024]{1,0:T(8,128)(2,1)} custom-call(bf16[128,768]{1,0:T(8,128)(2,1)} %ql_hbm.1, bf16[32,256]{1,0:T(8,128)(2,1)} %kl.1, bf16[32,64]{1,0:T(8,128)(2,1)} %rk.1, f32[6,128]{1,0:T(8,128)} %bitcast.3, f32[1,256]{1,0:T(1,128)} %bitcast.5, f32[1,512]{1,0:T(1,128)} %bitcast.4, f32[512,128]{1,0:T(8,128)} %constant.2.clone.table_hbm, ...), custom_call_target="tpu_custom_call" | custom-call | tf_op jit(solution)/shard_map/pallas_call | solution.py:522
  44.6 1.7 %copy.13 = bf16[128,1024]{1,0:T(8,128)(2,1)} copy(bf16[128,1024]{1,0:T(8,128)(2,1)} %shard_map.109) | data formatting | bytes 524288
